TPU v7x, 32 devices: a whole 2x2x4 slice. The times are simulated.
32 devices in a mesh: sp: 4 (over z), tp: 4 (over y, x), dp: 2 (over core).
Axes of the slice: x: 2, y: 2, z: 4, core: 2. Of those that a mesh axis runs over, the one named last changes fastest.
Arguments:
- latent: bfloat16 [2, 3072, 2048], P('dp', ('sp', 'tp')), may hold values from -3 to 3
- cond: bfloat16 [2, 2048], P('dp', 'sp'), may hold values from -6 to 6
- cond_ctx: bfloat16 [2048], P('sp'), may hold values from -6 to 6
- context: bfloat16 [2, 512, 2048], P('dp', 'sp'), may hold values from -6 to 6
- norm_gain: bfloat16 [2048], replicated, may hold values from 0.099609375 to 1.8984375
- mod_shift: bfloat16 [2048, 2048], P('sp', 'tp'), may hold values from -0.125 to 0.125
- mod_scale: bfloat16 [2048, 2048], P('sp', 'tp'), may hold values from -0.125 to 0.125
- mod_gate: bfloat16 [2048, 2048], P('sp', 'tp'), may hold values from -0.125 to 0.125
- w_query: bfloat16 [2048, 1024], P(None, 'tp'), may hold values from -0.125 to 0.125
- w_key: bfloat16 [2048, 256], P(None, 'tp'), may hold values from -0.125 to 0.125
- w_value: bfloat16 [2048, 256], P(None, 'tp'), may hold values from -0.125 to 0.125
- q_gain: bfloat16 [64], replicated, may hold values from 1 to 5.5
- k_gain: bfloat16 [64], replicated, may hold values from 1 to 5.5
- ctx_lift: float32 [16], P('tp'), may hold values from 1 to 3
- w_out: bfloat16 [1024, 2048], replicated, may hold values from -1.5 to 1.5
Outputs:
- mixed: bfloat16 [2, 3072, 2048], P('dp', ('sp', 'tp'))
All inputs are finite; a program needn't handle non-finite values.
Results may differ from a plain program's by a relative error of at most 0.009.
The roundings to bfloat16 on the way count: a program that leaves them out, or rounds other values in their place, can miss the bound.
Values may be sent and summed in bfloat16 or wider, within the bound.
A program may use at most 64 MiB of HBM per device.

v0:
```python
import jax
import jax.numpy as jnp
from jax import lax
from jax.sharding import PartitionSpec as P

HD = 64
GRID_W = 128
EPS = 1e-06
THETA = 10000.0


def modulate(row_block, gain_vec, shift_rows, scale_rows):
    values = row_block.astype(jnp.float32)
    normed = (
        values
        * lax.rsqrt(jnp.mean(values * values, axis=-1, keepdims=True) + EPS)
        * gain_vec.astype(jnp.float32)
    )
    return (normed * (1.0 + scale_rows) + shift_rows).astype(jnp.bfloat16)


def head_norm(raw_proj, gain_vec):
    samples, tokens, width = raw_proj.shape
    pieces = raw_proj.reshape(samples, tokens, width // HD, HD)
    normed = (
        pieces
        * lax.rsqrt(jnp.mean(pieces * pieces, axis=-1, keepdims=True) + EPS)
        * gain_vec.astype(jnp.float32)
    )
    return normed.transpose(0, 2, 1, 3)


def rotate(vector, positions):
    pairs_count = vector.shape[-1] // 4
    grid_row = (positions // GRID_W).astype(jnp.float32)
    grid_col = (positions % GRID_W).astype(jnp.float32)
    inverse = THETA ** (-jnp.arange(pairs_count, dtype=jnp.float32) / pairs_count)
    angles = jnp.concatenate([grid_row[:, None] * inverse, grid_col[:, None] * inverse], axis=-1)
    cosine = jnp.cos(angles)
    sine_val = jnp.sin(angles)
    first_half = vector[..., 0::2]
    second_half = vector[..., 1::2]
    turned = jnp.stack(
        [
            first_half * cosine - second_half * sine_val,
            first_half * sine_val + second_half * cosine,
        ],
        axis=-1,
    )
    return turned.reshape(vector.shape)


def split_heads(rows):
    samples, tokens, width = rows.shape
    return rows.reshape(samples, tokens, width // HD, HD).transpose(0, 2, 1, 3)


def on_device(
    latent,
    cond,
    cond_ctx,
    context,
    norm_gain,
    mod_shift,
    mod_scale,
    mod_gate,
    w_query,
    w_key,
    w_value,
    q_gain,
    k_gain,
    ctx_lift,
    w_out,
):
    samples = latent.shape[0]
    active = jax.nn.silu(
        jnp.concatenate([cond, cond_ctx[None, :]], axis=0).astype(jnp.float32)
    ).astype(jnp.bfloat16)
    partial_mods = tuple(
        (
            jnp.dot(active, weight, preferred_element_type=jnp.float32)
            for weight in (mod_shift, mod_scale, mod_gate)
        )
    )
    summed = lax.psum(partial_mods, "sp")
    shift_rows, scale_rows, gate_rows = lax.all_gather(summed, "tp", axis=1, tiled=True)
    modulated = modulate(
        latent, norm_gain, shift_rows[:samples, None, :], scale_rows[:samples, None, :]
    )
    ctx_mod = modulate(context, norm_gain, shift_rows[samples], scale_rows[samples])
    q_width = w_query.shape[1]
    k_width = w_key.shape[1]
    w_joint = jnp.concatenate([w_query, w_key, w_value], axis=1)
    projected = jnp.einsum(
        "srd,dc->src",
        lax.all_gather(modulated, "tp", axis=1, tiled=True),
        w_joint,
        preferred_element_type=jnp.float32,
    )
    tokens = projected.shape[1]
    k_heads = k_width // HD
    group_size = q_width // k_width
    positions = lax.axis_index("sp") * tokens + jnp.arange(tokens, dtype=jnp.int32)
    queries = rotate(head_norm(projected[..., :q_width], q_gain), positions).astype(jnp.bfloat16)
    queries = queries.reshape(samples, k_heads, group_size, tokens, HD)
    key_rows = rotate(
        head_norm(projected[..., q_width : q_width + k_width], k_gain), positions
    ).astype(jnp.bfloat16)
    value_rows = split_heads(projected[..., q_width + k_width :].astype(jnp.bfloat16))
    ctx_proj = jnp.einsum(
        "srd,dc->src", ctx_mod, w_joint[:, q_width:], preferred_element_type=jnp.float32
    )
    ctx_keys = head_norm(ctx_proj[..., :k_width], k_gain).astype(jnp.bfloat16)
    ctx_values = split_heads(ctx_proj[..., k_width:].astype(jnp.bfloat16))
    lift_table = ctx_lift.reshape(1, k_heads, group_size, 1, 1)
    factor = HD ** (-0.5)

    def absorb(state_now, key_block, value_block, score_lift):
        best_old, weight_sum, accumulated = state_now
        scores = (
            jnp.einsum("skgtd,skrd->skgtr", queries, key_block, preferred_element_type=jnp.float32)
            * factor
            + score_lift
        )
        peak = jnp.maximum(best_old, jnp.max(scores, axis=-1))
        weights = jnp.exp(scores - peak[..., None])
        rescale = jnp.exp(best_old - peak)
        weight_sum = weight_sum * rescale + jnp.sum(weights, axis=-1)
        accumulated = accumulated * rescale[..., None] + jnp.einsum(
            "skgtr,skrd->skgtd",
            weights.astype(jnp.bfloat16),
            value_block,
            preferred_element_type=jnp.float32,
        )
        return (peak, weight_sum, accumulated)

    stat_shape = (samples, k_heads, group_size, tokens)
    state_now = (
        jnp.full(stat_shape, -1e30, jnp.float32),
        jnp.zeros(stat_shape, jnp.float32),
        jnp.zeros(stat_shape + (HD,), jnp.float32),
    )
    all_ctx_keys, all_ctx_values = (
        lax.all_gather(ctx_keys, "sp", axis=2, tiled=True),
        lax.all_gather(ctx_values, "sp", axis=2, tiled=True),
    )
    state_now = absorb(state_now, all_ctx_keys, all_ctx_values, lift_table)
    key_piece = lax.all_gather(key_rows, "sp", axis=2, tiled=True)
    value_piece = lax.all_gather(value_rows, "sp", axis=2, tiled=True)
    block_count = key_piece.shape[2] // tokens
    key_blocks = jnp.moveaxis(key_piece.reshape(samples, k_heads, block_count, tokens, HD), 2, 0)
    value_blocks = jnp.moveaxis(
        value_piece.reshape(samples, k_heads, block_count, tokens, HD), 2, 0
    )

    def step_block(carry, blocks):
        return (absorb(carry, blocks[0], blocks[1], 0.0), None)

    state_out, unused = lax.scan(step_block, state_now, (key_blocks, value_blocks))
    state_now = state_out
    best_old, weight_sum, accumulated = state_now
    attended = (accumulated / weight_sum[..., None]).astype(jnp.bfloat16)
    head_rows = attended.transpose(0, 3, 1, 2, 4).reshape(samples, tokens, q_width)
    projected_out = jnp.einsum(
        "srq,qd->srd",
        lax.all_to_all(head_rows, "tp", split_axis=1, concat_axis=2, tiled=True),
        w_out,
        preferred_element_type=jnp.float32,
    )
    return (latent.astype(jnp.float32) + gate_rows[:samples, None, :] * projected_out).astype(
        jnp.bfloat16
    )


def solution(mesh):
    placed = (
        P("dp", ("sp", "tp"), None),
        P("dp", "sp"),
        P("sp"),
        P("dp", "sp", None),
        P(),
        P("sp", "tp"),
        P("sp", "tp"),
        P("sp", "tp"),
        P(None, "tp"),
        P(None, "tp"),
        P(None, "tp"),
        P(),
        P(),
        P("tp"),
        P(),
    )
    return jax.shard_map(
        on_device,
        mesh=mesh,
        in_specs=placed,
        out_specs=P("dp", ("sp", "tp"), None),
        check_vma=False,
    )
```

profile of v0, /device:TPU:0, one launch (start us, length us, event | category | flops | bytes accessed | tf_op | source)
XLA Modules:
  0.0 190.3 jit_solution(14167755606228791362)
XLA Ops:
  6.6 0.8 broadcast_in_dim.10
  7.4 0.2 copy-done
  7.6 0.8 fusion.94
  8.4 1.2 fusion.96
  9.7 1.2 fusion.98
  10.9 20.5 %all-reduce = (f32[2,512]{1,0:T(2,128)S(1)}, f32[2,512]{1,0:T(2,128)S(1)}, f32[2,512]{1,0:T(2,128)S(1)}) all-reduce(f32[2,512]{1,0:T(2,128)S(1)} %fusion.94, f32[2,512]{1,0:T(2,128)S(1)} %fusion.96, f32[2,512]{1,0:T(2,128)S(1)} %fusion.98), channel_id=1, replica_groups=mesh['sp'=4,'tp'=4,'dp'=2] {'sp'}, use_global_device_ids=true, to_apply=%region_3.4 | all-reduce | flops 3072 | bytes 24576 | tf_op jit(solution)/shard_map/psum | solution.py:85
  31.4 8.2 %all_gather.25 = f32[2,2048]{1,0:T(2,128)S(1)} all-gather(f32[2,512]{1,0:T(2,128)S(1)} %get-tuple-element.88), channel_id=1, replica_groups=mesh['sp'=4,'tp'=4,'dp'=2] {'tp'}, dimensions={1}, use_global_device_ids=true | all-gather | bytes 20480 | tf_op jit(solution)/shard_map/all_gather | solution.py:86
  39.6 8.2 %all_gather.26 = f32[2,2048]{1,0:T(2,128)S(1)} all-gather(f32[2,512]{1,0:T(2,128)S(1)} %get-tuple-element.87), channel_id=1, replica_groups=mesh['sp'=4,'tp'=4,'dp'=2] {'tp'}, dimensions={1}, use_global_device_ids=true | all-gather | bytes 20480 | tf_op jit(solution)/shard_map/all_gather | solution.py:86
  47.7 0.7 convert_element_type.119
  48.4 1.4 fusion.31
  49.8 2.4 %fusion.35 = bf16[1,192,2048]{2,1,0:T(8,128)(2,1)} fusion(bf16[1,192,2048]{2,1,0:T(8,128)(2,1)} %param.17, f32[2048]{0:T(1024)S(1)} %bitcast.173, f32[2048]{0:T(1024)S(1)} %bitcast.172, f32[2048]{0:T(1024)S(1)} %convert_element_type.119, f32[192]{0:T(256)S(1)} %add_rsqrt_fusion.2), kind=kLoop, calls=%fused_computation.39 | loop fusion | flops 2359296 | bytes 1598208 | tf_op jit(solution)/shard_map/convert_element_type | solution.py:19
  52.2 0.3 copy.46
  52.5 0.3 copy.47
  52.9 0.2 fusion.52
  53.1 0.4 convolution_bitcast_fusion
  53.6 0.1 fusion.77
  53.6 12.0 %all_gather.28 = bf16[1,1,512,64]{2,3,1,0:T(8,128)(2,1)S(1)} all-gather(bf16[1,1,128,64]{2,3,1,0:T(8,128)(2,1)S(1)} %fusion.77), channel_id=1, replica_groups=mesh['sp'=4,'tp'=4,'dp'=2] {'sp'}, dimensions={2}, use_global_device_ids=true | all-gather | bytes 81920 | tf_op jit(solution)/shard_map/all_gather | solution.py:144
  65.7 12.6 %all-gather = bf16[1,512,64]{1,2,0:T(8,128)(2,1)} all-gather(bf16[1,128,64]{1,2,0:T(8,128)(2,1)S(1)} %slice.80), channel_id=2, replica_groups=mesh['sp'=4,'tp'=4,'dp'=2] {'sp'}, dimensions={1}, use_global_device_ids=true | all-gather | bytes 81920 | tf_op jit(solution)/shard_map/all_gather | solution.py:145
  78.3 0.7 fusion.78
  79.0 1.0 fusion.70
  80.1 13.4 %all-gather.4.cloned.1.call-done = bf16[1,768,2048]{2,1,0:T(8,128)(2,1)} async-done(((bf16[1,192,2048]{2,1,0:T(8,128)(2,1)}), bf16[1,768,2048]{2,1,0:T(8,128)(2,1)}) %all-gather.4.cloned.1.call-update) | async-done | bytes 3145744 | tf_op jit(solution)/shard_map/all_gather | solution.py:96
  93.5 3.7 %fusion.41 = f32[1,768,384]{1,2,0:T(8,128)S(1)} fusion(bf16[2048,64]{1,0:T(8,128)(2,1)S(1)} %copy.47, bf16[2048,64]{1,0:T(8,128)(2,1)S(1)} %copy.46, bf16[2048,256]{1,0:T(8,128)(2,1)} %param.25, bf16[1,768,2048]{2,1,0:T(8,128)(2,1)} %all-gather.4.cloned.1.call-done), kind=kOutput, calls=%fused_computation.45 | convolution fusion | flops 1212678144 | bytes 5898240 | tf_op jit(solution)/shard_map/srd,dc->src/dot_general | solution.py:94
  97.2 0.1 fusion.66
  97.4 0.1 multiply_reduce_fusion
  97.5 0.1 multiply_bitcast_fusion
  97.7 0.2 slice.50
  97.9 0.2 slice.51
  98.1 1.0 subtract_bitcast_fusion
  99.2 0.4 copy.48
  99.6 0.1 convert_element_type.125
  99.7 0.1 convert_element_type.132
  99.9 1.2 fusion.74
  101.1 0.1 copy.50
  101.3 14.6 %all_gather.30 = bf16[1,1,3072,64]{2,3,1,0:T(8,128)(2,1)S(1)} all-gather(bf16[1,1,768,64]{2,3,1,0:T(8,128)(2,1)S(1)} %convert_element_type.131), channel_id=1, replica_groups=mesh['sp'=4,'tp'=4,'dp'=2] {'sp'}, dimensions={2}, use_global_device_ids=true | all-gather | bytes 491520 | tf_op jit(solution)/shard_map/all_gather | solution.py:148
  115.9 1.1 fusion.21
  117.0 2.6 %copy-done.1 = f32[4,768,512]{1,2,0:T(8,128)} copy-done((f32[4,768,512]{1,2,0:T(8,128)}, f32[4,768,512]{1,2,0:T(8,128)S(1)}, u32[]{:S(2)}) %copy-start.1) | copy-done | bytes 6291480
  119.6 1.3 fusion.23
  120.9 15.5 %all-gather.1 = bf16[1,3072,64]{1,2,0:T(8,128)(2,1)S(1)} all-gather(bf16[1,768,64]{1,2,0:T(8,128)(2,1)S(1)} %slice.79), channel_id=3, replica_groups=mesh['sp'=4,'tp'=4,'dp'=2] {'sp'}, dimensions={1}, use_global_device_ids=true | all-gather | bytes 491520 | tf_op jit(solution)/shard_map/all_gather | solution.py:149
  136.4 0.3 transpose_reshape.15
  136.8 4.3 %fusion.49 = f32[1,1,4,768,64]{3,4,2,1,0:T(8,128)S(1)} fusion(f32[4,768,512]{1,2,0:T(8,128)} %copy-done.1, f32[4,768]{1,0:T(4,128)S(1)} %get-tuple-element.106, f32[4]{0:T(128)S(1)} %copy-done.7, f32[4,768]{1,0:T(4,128)S(1)} %get-tuple-element.104, bf16[1,512,64]{1,2,0:T(8,128)(2,1)S(1)} %copy-done.6), kind=kOutput, calls=%fused_computation.49 | convolution fusion | flops 207814656 | bytes 7168016 | tf_op jit(solution)/shard_map/skgtr,skrd->skgtd/dot_general | solution.py:129
  141.0 19.7 %while.14 = (s32[]{:T(128)}, f32[1,1,4,768]{3,2,1,0:T(4,128)S(1)}, f32[1,1,4,768]{3,2,1,0:T(4,128)S(1)}, f32[1,1,4,768,64]{3,4,2,1,0:T(8,128)S(1)}, bf16[4,1,1,7...) while((s32[]{:T(128)}, f32[1,1,4,768]{3,2,1,0:T(4,128)S(1)}, ...), condition=%wide.region_13.14_spmd, body=%wide.region_10.13_spmd.sunk | while | flops 623256576 | bytes 30670940 | solution.py:159
  141.1 1.4 bitcast_reduce_fusion.2
  142.5 1.9 fusion.116
  144.4 1.6 fusion.115
  146.0 1.4 bitcast_reduce_fusion.2
  147.4 1.9 fusion.116
  149.3 1.6 fusion.115
  150.9 1.4 bitcast_reduce_fusion.2
  152.4 1.9 fusion.116
  154.3 1.6 fusion.115
  155.9 1.4 bitcast_reduce_fusion.2
  157.3 1.9 fusion.116
  159.2 1.6 fusion.115
  160.8 0.1 divide_convert_fusion
  160.9 0.6 copy.54
  161.5 0.5 broadcast.433
  162.0 3.0 %reduce.15 = bf16[768,256]{1,0:T(8,128)(2,1)S(1)} reduce(bf16[768,1,256]{2,1,0:T(2,128)(2,1)S(1)} %bitcast.162, bf16[]{:T(256)} %broadcast.433), dimensions={1}, to_apply=%bitcast.124.reduce_sub_computation | reduce | bytes 786434
  165.0 0.8 reshape.683
  165.9 3.5 %all-to-all-start = ((bf16[4,2,24576]{2,1,0:T(2,128)(2,1)}), bf16[4,2,24576]{2,1,0:T(2,128)(2,1)S(1)}, u32[]{:S(2)}, u32[]{:S(2)}) async-start(bf16[4,2,24576]{2,1,0:T(2,128)(2,1)} %reshape.683), calls=%async_computation | async-start | bytes 786432 | tf_op jit(solution)/shard_map/all_to_all | solution.py:166
  169.4 9.1 %all_gather.24 = f32[2,2048]{1,0:T(2,128)S(1)} all-gather(f32[2,512]{1,0:T(2,128)S(1)} %get-tuple-element.89), channel_id=1, replica_groups=mesh['sp'=4,'tp'=4,'dp'=2] {'tp'}, dimensions={1}, use_global_device_ids=true | all-gather | bytes 20480 | tf_op jit(solution)/shard_map/all_gather | solution.py:86
  178.4 0.4 reshape.684
  178.9 0.1 copy.58
  178.9 0.3 copy.55
  179.3 4.1 %fusion.30 = bf16[1,192,2048]{2,1,0:T(8,128)(2,1)} fusion(bf16[192,1024]{1,0:T(8,128)(2,1)S(1)} %bitcast.171, bf16[1024,2048]{1,0:T(8,128)(2,1)} %param.31, bf16[1,192,2048]{2,1,0:T(8,128)(2,1)S(1)} %copy-done.2, f32[2048]{0:T(1024)S(1)} %bitcast.174), kind=kOutput, calls=%fused_computation.32 | convolution fusion | flops 806879232 | bytes 6168576 | tf_op jit(solution)/shard_map/srq,qd->srd/dot_general | solution.py:164
  (60 shorter events, 0.8 us)
Async XLA Ops:
  6.5 1.0 copy-start
  6.5 45.7 %copy-start.5 = (bf16[2048,64]{0,1:T(8,128)(2,1)S(1)}, bf16[2048,64]{0,1:T(8,128)(2,1)}, u32[]{:S(2)}) copy-start(bf16[2048,64]{0,1:T(8,128)(2,1)} %param.26) | copy-start | bytes 786436
  6.5 46.0 %copy-start.4 = (bf16[2048,64]{0,1:T(8,128)(2,1)S(1)}, bf16[2048,64]{0,1:T(8,128)(2,1)}, u32[]{:S(2)}) copy-start(bf16[2048,64]{0,1:T(8,128)(2,1)} %param.27) | copy-start | bytes 786436
  6.5 46.3 %copy-start.8 = (bf16[64]{0:T(256)(128)(2,1)S(1)}, bf16[64]{0:T(256)(128)(2,1)}, u32[]{:S(2)}) copy-start(bf16[64]{0:T(256)(128)(2,1)} %param.29) | copy-start | bytes 388
  6.5 46.3 %copy-start.9 = (bf16[64]{0:T(256)(128)(2,1)S(1)}, bf16[64]{0:T(256)(128)(2,1)}, u32[]{:S(2)}) copy-start(bf16[64]{0:T(256)(128)(2,1)} %param.28) | copy-start | bytes 388
  6.5 46.3 %copy-start.3 = (bf16[1,128,2048]{2,1,0:T(8,128)(2,1)S(1)}, bf16[1,128,2048]{2,1,0:T(8,128)(2,1)}, u32[]{:S(2)}) copy-start(bf16[1,128,2048]{2,1,0:T(8,128)(2,1)} %param.20) | copy-start | bytes 1572868
  6.6 86.9 %all-gather.4.cloned.1.call-start = ((), (), s32[]{:S(2)}) async-start(), calls=%async_computation.1 | async-start | bytes 3932160 | tf_op jit(solution)/shard_map/all_gather | solution.py:96
  97.5 18.4 %copy-start.7 = (f32[4]{0:T(128)S(1)}, f32[4]{0:T(128)}, u32[]{:S(2)}) copy-start(f32[4]{0:T(128)} %param.30) | copy-start | bytes 52
  116.9 2.7 %copy-start.1 = (f32[4,768,512]{1,2,0:T(8,128)}, f32[4,768,512]{1,2,0:T(8,128)S(1)}, u32[]{:S(2)}) copy-start(f32[4,768,512]{1,2,0:T(8,128)S(1)} %get-tuple-element.114) | copy-start | bytes 18874372
  117.0 19.8 %copy-start.6 = (bf16[1,512,64]{1,2,0:T(8,128)(2,1)S(1)}, bf16[1,512,64]{1,2,0:T(8,128)(2,1)}, u32[]{:S(2)}) copy-start(bf16[1,512,64]{1,2,0:T(8,128)(2,1)} %all-gather) | copy-start | bytes 196612
  160.8 18.5 %copy-start.2 = (bf16[1,192,2048]{2,1,0:T(8,128)(2,1)S(1)}, bf16[1,192,2048]{2,1,0:T(8,128)(2,1)}, u32[]{:S(2)}) copy-start(bf16[1,192,2048]{2,1,0:T(8,128)(2,1)} %param.17) | copy-start | bytes 2359300
  165.9 12.5 %all-to-all-start = ((bf16[4,2,24576]{2,1,0:T(2,128)(2,1)}), bf16[4,2,24576]{2,1,0:T(2,128)(2,1)S(1)}, u32[]{:S(2)}, u32[]{:S(2)}) async-start(bf16[4,2,24576]{2,1,0:T(2,128)(2,1)} %reshape.683), calls=%async_computation | async-start | bytes 786432 | tf_op jit(solution)/shard_map/all_to_all | solution.py:166
Sparse Core Ops, SparseCore 0:
  52.3 41.0 all-gather.3
where the time goes:
time: 191 us; the launch traced here: 190 us
  blocking collectives  101 us (53%)
  matrix products  30 us (16%)
  other arithmetic  20 us (10%)
  between operations  13.8 us (7%)
  waiting for transfers between devices  13.4 us (7%)
  local copies, waits for them, and re-layouts  8.75 us (5%)
  starting transfers between devices  3.5 us (2%)
    all_gather x3, blocking collectives, on_device(): lax.all_gather(summed, 'tp', axis=1, tiled=True)  25.4 us
    psum x1, blocking collectives, on_device(): summed = lax.psum(partial_mods, 'sp')  20.5 us
    all_gather x1, blocking collectives, on_device(): value_piece = lax.all_gather(value_rows, 'sp', axis=2, tiled=True)  15.5 us
    all_gather x1, blocking collectives, on_device(): key_piece = lax.all_gather(key_rows, 'sp', axis=2, tiled=True)  14.6 us
    all_gather x1, waiting for transfers between devices, on_device(): lax.all_gather(modulated, 'tp', axis=1, tiled=True)  13.4 us
    all_gather x1, blocking collectives, on_device(): lax.all_gather(ctx_values, 'sp', axis=2, tiled=True)  12.6 us
    all_gather x1, blocking collectives, on_device(): lax.all_gather(ctx_keys, 'sp', axis=2, tiled=True)  12 us
    dot_general x5, matrix products, absorb(): jnp.einsum('skgtr,skrd->skgtd', weights.astype(jnp.bfloat16), value_block...  11.7 us
  transfers between devices with their start and end apart: 2, of which 1 were waited for; matrix products, arithmetic and copies ran while one was open for 2% of the time, Pallas kernels for 0%

commit v1 on v0

--- a/solution.py
+++ b/solution.py
@@ -7,6 +7,12 @@
 GRID_W = 128
 EPS = 1e-06
 THETA = 10000.0
+
+
+def laid_out(blocks, dim):
+    shape = list(blocks.shape[1:])
+    shape[dim] *= blocks.shape[0]
+    return jnp.moveaxis(blocks, 0, dim).reshape(shape)
 
 
 def modulate(row_block, gain_vec, shift_rows, scale_rows):
@@ -91,12 +97,18 @@
     q_width = w_query.shape[1]
     k_width = w_key.shape[1]
     w_joint = jnp.concatenate([w_query, w_key, w_value], axis=1)
-    projected = jnp.einsum(
-        "srd,dc->src",
-        lax.all_gather(modulated, "tp", axis=1, tiled=True),
-        w_joint,
-        preferred_element_type=jnp.float32,
-    )
+    size, index, extent = (lax.axis_size("tp"), lax.axis_index("tp"), modulated.shape[1])
+    right = [(i, (i + 1) % size) for i in range(size)]
+    blocks_2 = []
+    held = modulated
+    for step in range(size):
+        following = held if step == size - 1 else lax.ppermute(held, "tp", right)
+        blocks_2.append(
+            jnp.einsum("srd,dc->src", held, w_joint, preferred_element_type=jnp.float32)
+        )
+        held = following
+    blocks_2 = jnp.stack(blocks_2)[(index - jnp.arange(size)) % size]
+    projected = laid_out(blocks_2, 1)
     tokens = projected.shape[1]
     k_heads = k_width // HD
     group_size = q_width // k_width

time: 191 us -> 192 us (level)
  between operations: 13.8 us -> 0.56 us
  waiting for transfers between devices: 13.4 us -> 25.1 us
  starting transfers between devices: 3.5 us -> 5.49 us
    ppermute x0 -> x3, waiting for transfers between devices: none -> 25.1 us  [on_device(): following = held if step == size - 1 else lax.ppermute(held, 'tp', right)]
    all_gather x1 -> x0, waiting for transfers between devices: 13.4 us -> none  [on_device(): lax.all_gather(modulated, 'tp', axis=1, tiled=True)]
    ppermute x0 -> x3, starting transfers between devices: none -> 2.03 us  [on_device(): following = held if step == size - 1 else lax.ppermute(held, 'tp', right)]
    dot_general x1 -> x4, matrix products: 3.66 us -> 5.26 us  [on_device(): jnp.einsum('srd,dc->src', held, w_joint, preferred_element_type=jnp.float32)]
    unnamed x27 -> x36, local copies, waits for them, and re-layouts: 5.28 us -> 4.57 us
  transfers between devices with their start and end apart: 2 -> 4, of which waited for: 1 -> 2; matrix products, arithmetic and copies ran while one was open for 2% -> 4% of each run, Pallas kernels for 0% -> 0%
where the time goes in v1:
time: 192 us; the launch traced here: 191 us
  blocking collectives  101 us (53%)
  matrix products  31.6 us (16%)
  waiting for transfers between devices  25.1 us (13%)
  other arithmetic  18.4 us (10%)
  local copies, waits for them, and re-layouts  9.01 us (5%)
  starting transfers between devices  5.49 us (3%)
    all_gather x3, blocking collectives, on_device(): lax.all_gather(summed, 'tp', axis=1, tiled=True)  25.5 us
    ppermute x3, waiting for transfers between devices, on_device(): following = held if step == size - 1 else lax.ppermute(held, 'tp', right)  25.1 us
    psum x1, blocking collectives, on_device(): summed = lax.psum(partial_mods, 'sp')  20.5 us
    all_gather x1, blocking collectives, on_device(): key_piece = lax.all_gather(key_rows, 'sp', axis=2, tiled=True)  15.3 us
    all_gather x1, blocking collectives, on_device(): value_piece = lax.all_gather(value_rows, 'sp', axis=2, tiled=True)  14.6 us
    all_gather x1, blocking collectives, on_device(): lax.all_gather(ctx_values, 'sp', axis=2, tiled=True)  12.6 us
    all_gather x1, blocking collectives, on_device(): lax.all_gather(ctx_keys, 'sp', axis=2, tiled=True)  12.1 us
    dot_general x5, matrix products, absorb(): jnp.einsum('skgtr,skrd->skgtd', weights.astype(jnp.bfloat16), value_block...  11.7 us
  transfers between devices with their start and end apart: 4, of which 2 were waited for; matrix products, arithmetic and copies ran while one was open for 4% of the time, Pallas kernels for 0%

profile of v1, /device:TPU:0, one launch (start us, length us, event | category | flops | bytes accessed | tf_op | source)
XLA Modules:
  0.0 191.1 jit_solution(13506472082440747713)
XLA Ops:
  0.0 0.8 broadcast_in_dim.10
  0.8 0.2 copy-done
  1.1 0.8 fusion.87
  1.9 1.2 fusion.89
  3.1 1.2 fusion.91
  4.4 20.5 %all-reduce = (f32[2,512]{1,0:T(2,128)S(1)}, f32[2,512]{1,0:T(2,128)S(1)}, f32[2,512]{1,0:T(2,128)S(1)}) all-reduce(f32[2,512]{1,0:T(2,128)S(1)} %fusion.87, f32[2,512]{1,0:T(2,128)S(1)} %fusion.89, f32[2,512]{1,0:T(2,128)S(1)} %fusion.91), channel_id=1, replica_groups=mesh['sp'=4,'tp'=4,'dp'=2] {'sp'}, use_global_device_ids=true, to_apply=%region_3.4 | all-reduce | flops 3072 | bytes 24576 | tf_op jit(solution)/shard_map/psum | solution.py:91
  24.8 8.2 %all_gather.22 = f32[2,2048]{1,0:T(2,128)S(1)} all-gather(f32[2,512]{1,0:T(2,128)S(1)} %get-tuple-element.81), channel_id=1, replica_groups=mesh['sp'=4,'tp'=4,'dp'=2] {'tp'}, dimensions={1}, use_global_device_ids=true | all-gather | bytes 20480 | tf_op jit(solution)/shard_map/all_gather | solution.py:92
  33.0 8.2 %all_gather.23 = f32[2,2048]{1,0:T(2,128)S(1)} all-gather(f32[2,512]{1,0:T(2,128)S(1)} %get-tuple-element.80), channel_id=1, replica_groups=mesh['sp'=4,'tp'=4,'dp'=2] {'tp'}, dimensions={1}, use_global_device_ids=true | all-gather | bytes 20480 | tf_op jit(solution)/shard_map/all_gather | solution.py:92
  41.3 0.7 convert_element_type.119
  42.0 1.4 fusion.29
  43.4 1.5 fusion.33
  44.9 0.6 collective-permute-start
  45.5 0.3 copy.53
  45.8 0.3 copy.54
  46.1 0.2 fusion.40
  46.3 0.5 convolution_bitcast_fusion.4
  46.9 12.1 %all_gather.24 = bf16[1,1,512,64]{2,3,1,0:T(8,128)(2,1)S(1)} all-gather(bf16[1,1,128,64]{2,3,1,0:T(8,128)(2,1)S(1)} %fusion.69), channel_id=1, replica_groups=mesh['sp'=4,'tp'=4,'dp'=2] {'sp'}, dimensions={2}, use_global_device_ids=true | all-gather | bytes 81920 | tf_op jit(solution)/shard_map/all_gather | solution.py:156
  59.0 12.6 %all-gather = bf16[1,512,64]{1,2,0:T(8,128)(2,1)} all-gather(bf16[1,128,64]{1,2,0:T(8,128)(2,1)S(1)} %slice.77), channel_id=2, replica_groups=mesh['sp'=4,'tp'=4,'dp'=2] {'sp'}, dimensions={1}, use_global_device_ids=true | all-gather | bytes 81920 | tf_op jit(solution)/shard_map/all_gather | solution.py:157
  71.6 1.4 collective-permute-start.1
  73.1 0.7 fusion.70
  73.8 1.0 fusion.62
  74.9 16.9 %collective-permute-done.1 = bf16[1,192,2048]{2,1,0:T(8,128)(2,1)S(1)} collective-permute-done((bf16[1,192,2048]{2,1,0:T(8,128)(2,1)}, bf16[1,192,2048]{2,1,0:T(8,128)(2,1)S(1)}, u32[]{:S(2)}, u32[]{:S(2)}) %collective-permute-start.1) | collective-permute-done | bytes 786464 | tf_op jit(solution)/shard_map/ppermute | solution.py:105
  91.8 1.8 convolution_bitcast_fusion.3
  93.7 2.2 %convolution_bitcast_fusion.2 = f32[1,1,192,384]{3,2,1,0:T(8,128)S(1)} fusion(bf16[1,192,2048]{2,1,0:T(8,128)(2,1)} %collective-permute-done, bf16[2048,64]{1,0:T(8,128)(2,1)S(1)} %copy.54, bf16[2048,64]{1,0:T(8,128)(2,1)S(1)} %copy.53, bf16[2048,256]{1,0:T(8,128)(2,1)} %param.25), kind=kOutput, calls=%fused_computation.47 | convolution fusion | flops 306708480 | bytes 2654208 | tf_op jit(solution)/shard_map/srd,dc->src/dot_general | solution.py:107
  95.8 0.6 convolution_bitcast_fusion.1
  96.5 8.2 %collective-permute-done.2 = bf16[1,192,2048]{2,1,0:T(8,128)(2,1)S(1)} collective-permute-done((bf16[1,192,2048]{2,1,0:T(8,128)(2,1)S(1)}, bf16[1,192,2048]{2,1,0:T(8,128)(2,1)S(1)}, u32[]{:S(2)}, u32[]{:S(2)}) %collective-permute-start.2) | collective-permute-done | bytes 786464 | tf_op jit(solution)/shard_map/ppermute | solution.py:105
  104.7 0.6 convolution_bitcast_fusion
  105.4 0.6 gather_fusion
  106.5 0.3 copy.70
  107.0 0.2 slice.50
  107.2 0.2 slice.51
  107.4 1.1 subtract_bitcast_fusion
  108.6 0.4 copy.56
  109.0 0.3 copy.60
  109.4 0.4 fusion.66
  110.0 15.3 %all_gather.26 = bf16[1,1,3072,64]{2,3,1,0:T(8,128)(2,1)S(1)} all-gather(bf16[1,1,768,64]{2,3,1,0:T(8,128)(2,1)S(1)} %convert_element_type.131), channel_id=1, replica_groups=mesh['sp'=4,'tp'=4,'dp'=2] {'sp'}, dimensions={2}, use_global_device_ids=true | all-gather | bytes 491520 | tf_op jit(solution)/shard_map/all_gather | solution.py:160
  125.5 1.1 fusion.21
  126.6 1.3 fusion.23
  127.9 1.3 copy-done.1
  129.4 14.6 %all-gather.1 = bf16[1,3072,64]{1,2,0:T(8,128)(2,1)S(1)} all-gather(bf16[1,768,64]{1,2,0:T(8,128)(2,1)S(1)} %copy.72), channel_id=3, replica_groups=mesh['sp'=4,'tp'=4,'dp'=2] {'sp'}, dimensions={1}, use_global_device_ids=true | all-gather | bytes 491520 | tf_op jit(solution)/shard_map/all_gather | solution.py:161
  144.0 0.3 transpose_reshape.15
  144.4 4.3 %fusion.37 = f32[1,1,4,768,64]{3,4,2,1,0:T(8,128)S(1)} fusion(f32[4,768,512]{1,2,0:T(8,128)} %copy-done.1, f32[4,768]{1,0:T(4,128)S(1)} %get-tuple-element.99, f32[4]{0:T(128)S(1)} %copy-done.9, f32[4,768]{1,0:T(4,128)S(1)} %get-tuple-element.97, bf16[1,512,64]{1,2,0:T(8,128)(2,1)S(1)} %copy-done.8), kind=kOutput, calls=%fused_computation.43 | convolution fusion | flops 207814656 | bytes 7168016 | tf_op jit(solution)/shard_map/skgtr,skrd->skgtd/dot_general | solution.py:141
  148.6 19.7 %while.14 = (s32[]{:T(128)}, f32[1,1,4,768]{3,2,1,0:T(4,128)S(1)}, f32[1,1,4,768]{3,2,1,0:T(4,128)S(1)}, f32[1,1,4,768,64]{3,4,2,1,0:T(8,128)S(1)}, bf16[4,1,1,7...) while((s32[]{:T(128)}, f32[1,1,4,768]{3,2,1,0:T(4,128)S(1)}, ...), condition=%wide.region_13.14_spmd, body=%wide.region_10.13_spmd.sunk | while | flops 623256576 | bytes 30670940 | solution.py:171
  148.6 1.4 bitcast_reduce_fusion.2
  150.1 1.9 fusion.109
  152.0 1.6 fusion.108
  153.6 1.4 bitcast_reduce_fusion.2
  155.0 1.9 fusion.109
  156.9 1.6 fusion.108
  158.5 1.4 bitcast_reduce_fusion.2
  160.0 1.9 fusion.109
  161.9 1.6 fusion.108
  163.5 1.4 bitcast_reduce_fusion.2
  164.9 1.9 fusion.109
  166.8 1.6 fusion.108
  168.5 0.6 copy.65
  169.1 0.5 broadcast.502
  169.6 3.1 %reduce.15 = bf16[768,256]{1,0:T(8,128)(2,1)S(1)} reduce(bf16[768,1,256]{2,1,0:T(2,128)(2,1)S(1)} %bitcast.183, bf16[]{:T(256)} %broadcast.502), dimensions={1}, to_apply=%bitcast.141.reduce_sub_computation | reduce | bytes 786434
  172.7 0.8 reshape.762
  173.5 3.5 %all-to-all-start = ((bf16[4,2,24576]{2,1,0:T(2,128)(2,1)}), bf16[4,2,24576]{2,1,0:T(2,128)(2,1)S(1)}, u32[]{:S(2)}, u32[]{:S(2)}) async-start(bf16[4,2,24576]{2,1,0:T(2,128)(2,1)} %reshape.762), calls=%async_computation | async-start | bytes 786432 | tf_op jit(solution)/shard_map/all_to_all | solution.py:178
  177.0 9.1 %all_gather.21 = f32[2,2048]{1,0:T(2,128)S(1)} all-gather(f32[2,512]{1,0:T(2,128)S(1)} %get-tuple-element.82), channel_id=1, replica_groups=mesh['sp'=4,'tp'=4,'dp'=2] {'tp'}, dimensions={1}, use_global_device_ids=true | all-gather | bytes 20480 | tf_op jit(solution)/shard_map/all_gather | solution.py:92
  186.1 0.4 reshape.763
  186.6 0.3 copy.66
  187.0 4.1 %fusion.28 = bf16[1,192,2048]{2,1,0:T(8,128)(2,1)} fusion(bf16[192,1024]{1,0:T(8,128)(2,1)S(1)} %bitcast.192, bf16[1024,2048]{1,0:T(8,128)(2,1)} %param.31, bf16[1,192,2048]{2,1,0:T(8,128)(2,1)S(1)} %copy-done.2, f32[2048]{0:T(1024)S(1)} %bitcast.195), kind=kOutput, calls=%fused_computation.31 | convolution fusion | flops 806879232 | bytes 6168576 | tf_op jit(solution)/shard_map/srq,qd->srd/dot_general | solution.py:176
  (81 shorter events, 2.1 us)
Async XLA Ops:
  0.0 1.1 copy-start
  0.0 45.5 %copy-start.5 = (bf16[2048,64]{0,1:T(8,128)(2,1)S(1)}, bf16[2048,64]{0,1:T(8,128)(2,1)}, u32[]{:S(2)}) copy-start(bf16[2048,64]{0,1:T(8,128)(2,1)} %param.26) | copy-start | bytes 786436
  0.0 45.8 %copy-start.4 = (bf16[2048,64]{0,1:T(8,128)(2,1)S(1)}, bf16[2048,64]{0,1:T(8,128)(2,1)}, u32[]{:S(2)}) copy-start(bf16[2048,64]{0,1:T(8,128)(2,1)} %param.27) | copy-start | bytes 786436
  0.0 46.1 %copy-start.11 = (bf16[64]{0:T(256)(128)(2,1)S(1)}, bf16[64]{0:T(256)(128)(2,1)}, u32[]{:S(2)}) copy-start(bf16[64]{0:T(256)(128)(2,1)} %param.29) | copy-start | bytes 388
  0.0 46.1 %copy-start.12 = (bf16[64]{0:T(256)(128)(2,1)S(1)}, bf16[64]{0:T(256)(128)(2,1)}, u32[]{:S(2)}) copy-start(bf16[64]{0:T(256)(128)(2,1)} %param.28) | copy-start | bytes 388
  0.0 46.1 %copy-start.3 = (bf16[1,128,2048]{2,1,0:T(8,128)(2,1)S(1)}, bf16[1,128,2048]{2,1,0:T(8,128)(2,1)}, u32[]{:S(2)}) copy-start(bf16[1,128,2048]{2,1,0:T(8,128)(2,1)} %param.20) | copy-start | bytes 1572868
  44.9 26.7 %collective-permute-start = (bf16[1,192,2048]{2,1,0:T(8,128)(2,1)S(1)}, bf16[1,192,2048]{2,1,0:T(8,128)(2,1)}, u32[]{:S(2)}, u32[]{:S(2)}) collective-permute-start(bf16[1,192,2048]{2,1,0:T(8,128)(2,1)S(1)} %fusion.33), channel_id=1, source_target_pairs={{0,2},{2,4},{4,6},{6,0},{1,3},{3,5},{5,7},{7,1},{8,10},{10,12},{12... | collective-permute-start | bytes 2359304 | tf_op jit(solution)/shard_map/ppermute | solution.py:105
  71.6 20.2 %collective-permute-start.1 = (bf16[1,192,2048]{2,1,0:T(8,128)(2,1)}, bf16[1,192,2048]{2,1,0:T(8,128)(2,1)S(1)}, u32[]{:S(2)}, u32[]{:S(2)}) collective-permute-start(bf16[1,192,2048]{2,1,0:T(8,128)(2,1)} %collective-permute-done), channel_id=1, source_target_pairs={{0,2},{2,4},{4,6},{6,0},{1,3},{3,5},{5,7},{7,1},{8,10},{10,12},{12... | collective-permute-start | bytes 2359304 | tf_op jit(solution)/shard_map/ppermute | solution.py:105
  91.8 12.9 %collective-permute-start.2 = (bf16[1,192,2048]{2,1,0:T(8,128)(2,1)S(1)}, bf16[1,192,2048]{2,1,0:T(8,128)(2,1)S(1)}, u32[]{:S(2)}, u32[]{:S(2)}) collective-permute-start(bf16[1,192,2048]{2,1,0:T(8,128)(2,1)S(1)} %collective-permute-done.1), channel_id=1, source_target_pairs={{0,2},{2,4},{4,6},{6,0},{1,3},{3,5},{5,7},{7,1},{8,10},{10,12},{12... | collective-permute-start | bytes 2359304 | tf_op jit(solution)/shard_map/ppermute | solution.py:105
  93.6 2.2 %copy-start.10 = (bf16[2048,256]{1,0:T(8,128)(2,1)S(1)}, bf16[2048,256]{1,0:T(8,128)(2,1)}, u32[]{:S(2)}) copy-start(bf16[2048,256]{1,0:T(8,128)(2,1)} %param.25) | copy-start | bytes 3145732
  107.4 2.0 %copy-start.6 = (f32[1,1,768,16]{2,3,1,0:T(8,128)S(1)}, f32[1,1,768,16]{2,3,1,0:T(8,128)}, u32[]{:S(2)}) copy-start(f32[1,1,768,16]{2,3,1,0:T(8,128)} %get-tuple-element.100) | copy-start | bytes 147460
  107.4 2.0 %copy-start.7 = (f32[1,1,768,16]{2,3,1,0:T(8,128)S(1)}, f32[1,1,768,16]{2,3,1,0:T(8,128)}, u32[]{:S(2)}) copy-start(f32[1,1,768,16]{2,3,1,0:T(8,128)} %get-tuple-element.105) | copy-start | bytes 147460
  108.5 17.0 %copy-start.9 = (f32[4]{0:T(128)S(1)}, f32[4]{0:T(128)}, u32[]{:S(2)}) copy-start(f32[4]{0:T(128)} %param.30) | copy-start | bytes 52
  126.6 2.7 %copy-start.1 = (f32[4,768,512]{1,2,0:T(8,128)}, f32[4,768,512]{1,2,0:T(8,128)S(1)}, u32[]{:S(2)}) copy-start(f32[4,768,512]{1,2,0:T(8,128)S(1)} %get-tuple-element.107) | copy-start | bytes 18874372
  129.2 15.1 %copy-start.8 = (bf16[1,512,64]{1,2,0:T(8,128)(2,1)S(1)}, bf16[1,512,64]{1,2,0:T(8,128)(2,1)}, u32[]{:S(2)}) copy-start(bf16[1,512,64]{1,2,0:T(8,128)(2,1)} %all-gather) | copy-start | bytes 196612
  169.6 17.4 %copy-start.2 = (bf16[1,192,2048]{2,1,0:T(8,128)(2,1)S(1)}, bf16[1,192,2048]{2,1,0:T(8,128)(2,1)}, u32[]{:S(2)}) copy-start(bf16[1,192,2048]{2,1,0:T(8,128)(2,1)} %param.17) | copy-start | bytes 2359300
  173.5 12.5 %all-to-all-start = ((bf16[4,2,24576]{2,1,0:T(2,128)(2,1)}), bf16[4,2,24576]{2,1,0:T(2,128)(2,1)S(1)}, u32[]{:S(2)}, u32[]{:S(2)}) async-start(bf16[4,2,24576]{2,1,0:T(2,128)(2,1)} %reshape.762), calls=%async_computation | async-start | bytes 786432 | tf_op jit(solution)/shard_map/all_to_all | solution.py:178
